TPU v7x, 512 devices: a whole 4x4x16 slice. The times are simulated.
512 devices in a mesh: fs: 16 (over y, x), tp: 32 (over z, core).
Axes of the slice: x: 4, y: 4, z: 16, core: 2. Of those that a mesh axis runs over, the one named last changes fastest.
Arguments:
- tokens: bfloat16 [8192, 2048], P('fs', 'tp'), may hold values from -6 to 6
- norm_gain: float32 [2048], P('fs'), may hold values from 0.1 to 1.9
- gate_train: float32 [2048, 8192], P('fs', 'tp'), may hold values from -0.125 to 0.125
- up_train: float32 [2048, 8192], P('fs', 'tp'), may hold values from -0.125 to 0.125
- down_train: float32 [8192, 2048], P('fs', 'tp'), may hold values from -0.0625 to 0.0625
Outputs:
- gate_serve: bfloat16 [2048, 8192], P(None, 'tp')
- up_serve: bfloat16 [2048, 8192], P(None, 'tp')
- down_serve: bfloat16 [8192, 2048], P('tp')
- layer_out: bfloat16 [8192, 2048], P(('fs', 'tp'))
All inputs are finite; a program needn't handle non-finite values.
Results may differ from a plain program's by a relative error of at most 0.024.
Values may be sent and summed in bfloat16 or wider, within the bound.
No kernel may reach another device: no remote copies, remote signals or barrier semaphores. Data moves between devices by JAX's collectives and lax.ppermute only.
A program may use at most 64 MiB of HBM per device.

v0:
```python
import jax
import jax.numpy as jnp
from jax import lax
from jax.sharding import Mesh
from jax.sharding import PartitionSpec as P

D = 2048
TP = ("tp_0", "tp_1")
FS_TP = ("fs", "tp_0", "tp_1")
epsilon = 1e-06


def side_by_side(arrays, axis, dim, along):
    both = jnp.concatenate(arrays, axis=along)
    whole, at, finished = (lax.all_gather(both, axis, axis=dim, tiled=True), 0, [])
    for a in arrays:
        finished.append(lax.slice_in_dim(whole, at, at + a.shape[along], axis=along))
        at += a.shape[along]
    return tuple(finished)


def joined_along(pieces, dim):
    shape = list(pieces.shape[1:])
    shape[dim] *= pieces.shape[0]
    return jnp.moveaxis(pieces, 0, dim).reshape(shape)


def copy_for_each(x, axis):
    copies = jnp.broadcast_to(x, (lax.axis_size(axis), *x.shape))
    return lax.all_to_all(copies, axis, split_axis=0, concat_axis=0, tiled=True)


def collect(x, axis, dim):
    return joined_along(copy_for_each(x, axis), dim)


def sum_in_order(pieces, axes, order):
    shape = [lax.axis_size(a) for a in axes]
    pieces = pieces.reshape(*shape, *pieces.shape[1:])
    pieces = pieces.transpose(*order, *range(len(axes), pieces.ndim))
    pieces = pieces.reshape(-1, *pieces.shape[len(axes) :])
    for k in order:
        pieces = lax.psum_scatter(pieces, axes[k], scatter_dimension=0, tiled=True)
    return pieces[0]


def cut_along(x, dim, count):
    before, after = (x.shape[:dim], x.shape[dim + 1 :])
    return jnp.moveaxis(x.reshape(*before, count, -1, *after), dim, 0)


def sum_by_axis(x, axes, order, dim):
    count = lax.axis_size(axes)
    return sum_in_order(cut_along(x, dim, count), axes, order)


def body(tokens, norm_gain, gate_train, up_train, down_train):
    gate_local = (norm_gain[:, None] * gate_train).astype(jnp.bfloat16)
    up_local = (norm_gain[:, None] * up_train).astype(jnp.bfloat16)
    down_local = down_train.astype(jnp.bfloat16)
    features = lax.all_gather(tokens, TP, axis=1, tiled=True)
    wide = features.astype(jnp.float32)
    squares = jnp.sum(wide * wide, axis=1)
    gate_whole, up_whole = side_by_side((gate_local, up_local), "fs", 0, 1)
    gate_sum = jnp.dot(features, gate_whole, preferred_element_type=jnp.float32)
    up_sum = jnp.dot(features, up_whole, preferred_element_type=jnp.float32)
    down_rows = collect(down_local, "fs", 0)
    down_whole = lax.all_to_all(down_rows, TP, split_axis=0, concat_axis=1, tiled=True)
    scale = lax.rsqrt(squares / D + epsilon)[:, None]
    hidden = (jax.nn.silu(gate_sum * scale) * (up_sum * scale)).astype(jnp.bfloat16)
    mixed = (
        sum_by_axis(
            jnp.dot(hidden, down_whole, preferred_element_type=jnp.float32).astype(jnp.bfloat16),
            TP,
            (1, 0),
            0,
        )
        .astype(jnp.float32)
        .astype(jnp.bfloat16)
    )
    return (gate_whole, up_whole, down_whole, mixed)


def solution(mesh):
    finer = Mesh(mesh.devices.reshape(mesh.shape["fs"], 16, 2), ("fs", "tp_0", "tp_1"))
    placed = (P("fs", TP), P("fs"), P("fs", TP), P("fs", TP), P("fs", TP))
    return jax.shard_map(
        body,
        mesh=finer,
        in_specs=placed,
        out_specs=(P(None, TP), P(None, TP), P(TP, None), P(FS_TP, None)),
        check_vma=False,
    )
```

profile of v0, /device:TPU:2, one launch (start us, length us, event | category | flops | bytes accessed | tf_op | source)
XLA Modules:
  0.0 262.0 jit_solution(8087558812155801704)
XLA Ops:
  7.2 0.0 all-gather.3.cloned.1.call-start
  7.2 1.1 multiply_convert_fusion.1
  8.3 0.7 pad_maximum_fusion
  9.0 0.9 convert_element_type.22
  9.9 1.1 broadcast_in_dim.2
  11.0 9.3 %all-to-all-start = ((bf16[16,512,64]{1,2,0:T(8,128)(2,1)}), bf16[16,512,64]{1,2,0:T(8,128)(2,1)S(1)}, u32[]{:S(2)}, u32[]{:S(2)}) async-start(bf16[16,512,64]{1,2,0:T(8,128)(2,1)} %broadcast_in_dim.2), calls=%async_computation | async-start | bytes 2097152 | tf_op jit(solution)/shard_map/all_to_all | solution.py:30
  20.3 0.7 all-gather.5.cloned.1.call-update
  21.0 13.6 %all-to-all-done = bf16[16,512,64]{1,2,0:T(8,128)(2,1)S(1)} async-done(((bf16[16,512,64]{1,2,0:T(8,128)(2,1)}), bf16[16,512,64]{1,2,0:T(8,128)(2,1)S(1)}, u32[]{:S(2)}, u32[]{:S(2)}) %all-to-all-start) | async-done | bytes 1048608 | tf_op jit(solution)/shard_map/all_to_all | solution.py:30
  34.7 0.6 copy.14
  35.2 0.4 all_to_all.18
  35.6 1.6 copy.15
  37.2 15.0 %all-to-all-start.1 = ((bf16[32,256,64]{1,2,0:T(8,128)(2,1)}), bf16[32,256,64]{1,2,0:T(8,128)(2,1)S(1)}, u32[]{:S(2)}, u32[]{:S(2)}) async-start(bf16[32,256,64]{1,2,0:T(8,128)(2,1)} %copy.15), calls=%async_computation.1 | async-start | bytes 2097152 | tf_op jit(solution)/shard_map/all_to_all | solution.py:68
  52.3 0.0 reduce-scatter.3.cloned.1.call-start
  52.3 23.6 %all-gather.3.cloned.1.call-done = bf16[2048,512]{1,0:T(8,128)(2,1)} async-done(((bf16[128,512]{1,0:T(8,128)(2,1)}), bf16[2048,512]{1,0:T(8,128)(2,1)}) %all-gather.3.cloned.1.call-update) | async-done | bytes 2097168 | tf_op jit(solution)/shard_map/all_gather | solution.py:15
  75.9 3.0 %fusion.12 = (bf16[2048,256]{1,0:T(8,128)(2,1)}, bf16[2048,256]{1,0:T(8,128)(2,1)}) fusion(bf16[2048,512]{1,0:T(8,128)(2,1)} %all-gather.3.cloned.1.call-done), kind=kLoop, calls=%fused_computation.20 | loop fusion | bytes 4194304 | tf_op jit(solution)/shard_map/slice | solution.py:17
  78.9 71.5 %all-gather.5.cloned.1.call-done = bf16[512,2048]{0,1:T(8,128)(2,1)} async-done(((bf16[512,64]{0,1:T(8,128)(2,1)}), bf16[512,2048]{0,1:T(8,128)(2,1)}) %all-gather.5.cloned.1.call-update) | async-done | bytes 2097168 | tf_op jit(solution)/shard_map/all_gather | solution.py:61
  150.4 2.2 multiply_reduce_fusion
  152.7 2.8 %fusion.2 = f32[512,256]{0,1:T(8,128)} fusion(bf16[2048,256]{1,0:T(8,128)(2,1)} %get-tuple-element.13, bf16[512,2048]{0,1:T(8,128)(2,1)S(1)} %copy-done, f32[512]{0:T(512)S(1)} %add_rsqrt_fusion), kind=kOutput, calls=%fused_computation.6 | convolution fusion | flops 537001984 | bytes 3672064 | tf_op jit(solution)/shard_map/dot_general | solution.py:65
  155.5 4.2 %convolution_convert_fusion = bf16[512,2048]{1,0:T(8,128)(2,1)} fusion(bf16[256,2048]{0,1:T(8,128)(2,1)S(1)} %bitcast.26, bf16[2048,256]{1,0:T(8,128)(2,1)} %get-tuple-element.12, bf16[512,2048]{0,1:T(8,128)(2,1)S(1)} %copy-done, f32[512,256]{0,1:T(8,128)} %fusion.2, f32[512]{0:T(512)S(1)} %add_rsqrt_fusion), kind=kOutput, calls=%fused_computation.1 | convolution fusion | flops 1075707904 | bytes 6817792 | tf_op jit(solution)/shard_map/dot_general | solution.py:73
  159.7 3.2 %copy.16 = bf16[2,16,16,2048]{3,2,1,0:T(8,128)(2,1)} copy(bf16[2,16,16,2048]{3,2,0,1:T(8,128)(2,1)} %bitcast.28) | data formatting | bytes 4194304 | tf_op jit(solution)/shard_map/transpose | solution.py:40
  162.8 0.0 reduce-scatter.5.cloned.1.call-start
  162.9 16.7 %reduce-scatter.3.cloned.1.call-done = bf16[16,16,2048]{2,1,0:T(8,128)(2,1)} async-done(((bf16[32,16,2048]{2,1,0:T(8,128)(2,1)}), bf16[16,16,2048]{2,1,0:T(8,128)(2,1)}) %reduce-scatter.3.cloned.1.call-update) | async-done | bytes 1048592 | tf_op jit(solution)/shard_map/reduce_scatter | solution.py:43
  179.6 1.4 copy.17
  181.0 74.5 %reduce-scatter.5.cloned.1.call-done = bf16[1,16,2048]{2,1,0:T(8,128)(2,1)} async-done(((bf16[16,16,2048]{2,1,0:T(8,128)(2,1)}), bf16[1,16,2048]{2,1,0:T(8,128)(2,1)}) %reduce-scatter.5.cloned.1.call-update) | async-done | bytes 65552 | tf_op jit(solution)/shard_map/reduce_scatter | solution.py:43
  (8 shorter events, 0.1 us)
Async XLA Ops:
  7.2 68.8 %all-gather.3.cloned.1.call-start = ((), (), s32[]{:S(2)}) async-start(), calls=%async_computation.4 | async-start | bytes 2228224 | tf_op jit(solution)/shard_map/all_gather | solution.py:15
  11.0 23.7 %all-to-all-start = ((bf16[16,512,64]{1,2,0:T(8,128)(2,1)}), bf16[16,512,64]{1,2,0:T(8,128)(2,1)S(1)}, u32[]{:S(2)}, u32[]{:S(2)}) async-start(bf16[16,512,64]{1,2,0:T(8,128)(2,1)} %broadcast_in_dim.2), calls=%async_computation | async-start | bytes 2097152 | tf_op jit(solution)/shard_map/all_to_all | solution.py:30
  20.3 130.1 %all-gather.5.cloned.1.call-start = ((), (), s32[]{:S(2)}) async-start(), calls=%async_computation.5 | async-start | bytes 2162688 | tf_op jit(solution)/shard_map/all_gather | solution.py:61
  37.2 118.3 %all-to-all-start.1 = ((bf16[32,256,64]{1,2,0:T(8,128)(2,1)}), bf16[32,256,64]{1,2,0:T(8,128)(2,1)S(1)}, u32[]{:S(2)}, u32[]{:S(2)}) async-start(bf16[32,256,64]{1,2,0:T(8,128)(2,1)} %copy.15), calls=%async_computation.1 | async-start | bytes 2097152 | tf_op jit(solution)/shard_map/all_to_all | solution.py:68
  52.3 127.3 %reduce-scatter.3.cloned.1.call-start = ((), (), s32[]{:S(2)}) async-start(), calls=%async_computation.6 | async-start | bytes 3145728 | tf_op jit(solution)/shard_map/reduce_scatter | solution.py:43
  150.4 2.3 copy-start
  162.8 92.6 %reduce-scatter.5.cloned.1.call-start = ((), (), s32[]{:S(2)}) async-start(), calls=%async_computation.7 | async-start | bytes 1114112 | tf_op jit(solution)/shard_map/reduce_scatter | solution.py:43
Sparse Core Ops, SparseCore 0:
  11.6 64.3 all-gather.2
  78.1 72.3 all-gather.4
  163.0 16.5 reduce-scatter.2
  182.8 72.6 reduce-scatter.4
where the time goes:
time: 262 us
  waiting for transfers between devices  201 us (77%)
  starting transfers between devices  24.5 us (9%)
  between operations  13.8 us (5%)
  local copies, waits for them, and re-layouts  11.2 us (4%)
  matrix products  6.97 us (3%)
  other arithmetic  4.91 us (2%)
    reduce_scatter x2, waiting for transfers between devices, sum_in_order(): pieces = lax.psum_scatter(pieces, axes[k], scatter_dimension=0, tiled=True)  91.2 us
    all_gather x1, waiting for transfers between devices, body(): features = lax.all_gather(tokens, TP, axis=1, tiled=True)  71.5 us
    all_gather x1, waiting for transfers between devices, side_by_side(): lax.all_gather(both, axis, axis=dim, tiled=True)  23.6 us
    all_to_all x1, starting transfers between devices, body(): lax.all_to_all(down_rows, TP, split_axis=0, concat_axis=1, tiled=True)  15 us
    all_to_all x1, waiting for transfers between devices, copy_for_each(): return lax.all_to_all(copies, axis, split_axis=0, concat_axis=0, tiled=True)  13.6 us
    all_to_all x1, starting transfers between devices, copy_for_each(): return lax.all_to_all(copies, axis, split_axis=0, concat_axis=0, tiled=True)  9.32 us
  transfers between devices with their start and end apart: 6, of which 5 were waited for; matrix products, arithmetic and copies ran while one was open for 5% of the time, Pallas kernels for 0%

commit v1 on v0

--- a/solution.py
+++ b/solution.py
@@ -58,7 +58,9 @@
     gate_local = (norm_gain[:, None] * gate_train).astype(jnp.bfloat16)
     up_local = (norm_gain[:, None] * up_train).astype(jnp.bfloat16)
     down_local = down_train.astype(jnp.bfloat16)
-    features = lax.all_gather(tokens, TP, axis=1, tiled=True)
+    features = jnp.concatenate(
+        lax.all_to_all(jnp.stack([tokens] * lax.axis_size(TP)), TP, 0, 0), axis=1
+    )
     wide = features.astype(jnp.float32)
     squares = jnp.sum(wide * wide, axis=1)
     gate_whole, up_whole = side_by_side((gate_local, up_local), "fs", 0, 1)

time: 262 us -> 308 us (1.18)
  waiting for transfers between devices: 201 us -> 228 us
  blocking collectives: 0 us -> 23.2 us
  starting transfers between devices: 24.5 us -> 20.4 us
    all_to_all x1, waiting for transfers between devices: 13.6 us -> 93.6 us  [body(): lax.all_to_all(jnp.stack([tokens] * lax.axis_size(TP)), TP, 0, 0)]
    all_gather x1 -> x0, waiting for transfers between devices: 71.5 us -> none  [body(): features = lax.all_gather(tokens, TP, axis=1, tiled=True)]
    all_to_all x1, waiting for transfers between devices: 0.01 us -> 50.8 us  [body(): lax.all_to_all(down_rows, TP, split_axis=0, concat_axis=1, tiled=True)]
    all_gather x1, waiting for transfers between devices: 23.6 us -> 0.02 us  [side_by_side(): lax.all_gather(both, axis, axis=dim, tiled=True)]
    all_to_all x0 -> x1, blocking collectives: none -> 23.2 us  [copy_for_each(): return lax.all_to_all(copies, axis, split_axis=0, concat_axis=0, tiled=True)]
    all_to_all x1, starting transfers between devices: 15 us -> 4.77 us  [body(): lax.all_to_all(down_rows, TP, split_axis=0, concat_axis=1, tiled=True)]
    reduce_scatter x2, waiting for transfers between devices: 91.2 us -> 83.9 us  [sum_in_order(): pieces = lax.psum_scatter(pieces, axes[k], scatter_dimension=0, tiled=True)]
    all_to_all x1, starting transfers between devices: 9.32 us -> 15.5 us  [body(): lax.all_to_all(jnp.stack([tokens] * lax.axis_size(TP)), TP, 0, 0)]
  transfers between devices with their start and end apart: 6 -> 5, of which waited for: 5 -> 4; matrix products, arithmetic and copies ran while one was open for 5% -> 3% of each run, Pallas kernels for 0% -> 0%
where the time goes in v1:
time: 308 us
  waiting for transfers between devices  228 us (74%)
  blocking collectives  23.2 us (8%)
  starting transfers between devices  20.4 us (7%)
  local copies, waits for them, and re-layouts  13.8 us (4%)
  between operations  13.8 us (4%)
  matrix products  5.72 us (2%)
    all_to_all x1, waiting for transfers between devices, body(): lax.all_to_all(jnp.stack([tokens] * lax.axis_size(TP)), TP, 0, 0)  93.6 us
    reduce_scatter x2, waiting for transfers between devices, sum_in_order(): pieces = lax.psum_scatter(pieces, axes[k], scatter_dimension=0, tiled=True)  83.9 us
    all_to_all x1, waiting for transfers between devices, body(): lax.all_to_all(down_rows, TP, split_axis=0, concat_axis=1, tiled=True)  50.8 us
    all_to_all x1, blocking collectives, copy_for_each(): return lax.all_to_all(copies, axis, split_axis=0, concat_axis=0, tiled=True)  23.2 us
    all_to_all x1, starting transfers between devices, body(): lax.all_to_all(jnp.stack([tokens] * lax.axis_size(TP)), TP, 0, 0)  15.5 us
  transfers between devices with their start and end apart: 5, of which 4 were waited for; matrix products, arithmetic and copies ran while one was open for 3% of the time, Pallas kernels for 0%

profile of v1, /device:TPU:2, one launch (start us, length us, event | category | flops | bytes accessed | tf_op | source)
XLA Modules:
  0.0 307.5 jit_solution(10498873877991649862)
XLA Ops:
  7.2 0.9 convert_element_type.23
  8.1 0.1 broadcast_in_dim.2
  8.2 23.2 %all_to_all.29 = bf16[16,512,64]{1,2,0:T(8,128)(2,1)S(1)} all-to-all(bf16[16,512,64]{1,2,0:T(8,128)(2,1)S(1)} %broadcast_in_dim.2), channel_id=1, replica_groups=mesh['fs'=16,'tp_0'=16,'tp_1'=2] {'fs'}, dimensions={0} | all-to-all | bytes 2097152 | tf_op jit(solution)/shard_map/all_to_all | solution.py:30
  31.4 1.6 stack.2
  32.9 15.5 %all-to-all-start.2 = ((bf16[32,512,64]{1,2,0:T(8,128)(2,1)}), bf16[32,512,64]{1,2,0:T(8,128)(2,1)S(1)}, u32[]{:S(2)}, u32[]{:S(2)}) async-start(bf16[32,512,64]{1,2,0:T(8,128)(2,1)} %stack.2), calls=%async_computation.2 | async-start | bytes 4194304 | tf_op jit(solution)/shard_map/all_to_all | solution.py:62
  48.5 0.1 multiply_convert_fusion.1
  48.6 0.7 pad_maximum_fusion
  49.3 1.5 copy.15
  50.9 1.4 all_to_all.21
  52.3 1.6 copy.16
  53.9 93.6 %all-to-all-done.2 = bf16[32,512,64]{1,2,0:T(8,128)(2,1)S(1)} async-done(((bf16[32,512,64]{1,2,0:T(8,128)(2,1)}), bf16[32,512,64]{1,2,0:T(8,128)(2,1)S(1)}, u32[]{:S(2)}, u32[]{:S(2)}) %all-to-all-start.2) | async-done | bytes 2097184 | tf_op jit(solution)/shard_map/all_to_all | solution.py:62
  147.4 4.8 %all-to-all-start.1 = ((bf16[32,256,64]{1,2,0:T(8,128)(2,1)}), bf16[32,256,64]{1,2,0:T(8,128)(2,1)S(1)}, u32[]{:S(2)}, u32[]{:S(2)}) async-start(bf16[32,256,64]{1,2,0:T(8,128)(2,1)} %copy.16), calls=%async_computation.1 | async-start | bytes 2097152 | tf_op jit(solution)/shard_map/all_to_all | solution.py:70
  152.2 0.0 reduce-scatter.3.cloned.1.call-start
  152.3 2.6 fusion.12
  154.9 0.6 multiply_reduce_fusion
  155.5 0.4 copy-done
  155.9 1.5 fusion.2
  157.4 50.8 %all-to-all-done.1 = bf16[32,256,64]{1,2,0:T(8,128)(2,1)S(1)} async-done(((bf16[32,256,64]{1,2,0:T(8,128)(2,1)}), bf16[32,256,64]{1,2,0:T(8,128)(2,1)S(1)}, u32[]{:S(2)}, u32[]{:S(2)}) %all-to-all-start.1) | async-done | bytes 1048608 | tf_op jit(solution)/shard_map/all_to_all | solution.py:70
  208.2 4.2 %convolution_convert_fusion = bf16[512,2048]{1,0:T(8,128)(2,1)} fusion(bf16[256,2048]{0,1:T(8,128)(2,1)S(1)} %bitcast.32, bf16[2048,256]{1,0:T(8,128)(2,1)} %get-tuple-element.12, bf16[512,2048]{0,1:T(8,128)(2,1)S(1)} %bitcast.30, f32[512,256]{0,1:T(8,128)} %fusion.2, f32[512]{0:T(512)S(1)} %add_rsqrt_fusion), kind=kOutput, calls=%fused_computation.1 | convolution fusion | flops 1075707904 | bytes 6817792 | tf_op jit(solution)/shard_map/dot_general | solution.py:75
  212.4 3.2 %copy.17 = bf16[2,16,16,2048]{3,2,1,0:T(8,128)(2,1)} copy(bf16[2,16,16,2048]{3,2,0,1:T(8,128)(2,1)} %bitcast.34) | data formatting | bytes 4194304 | tf_op jit(solution)/shard_map/transpose | solution.py:40
  215.6 0.0 reduce-scatter.5.cloned.1.call-start
  215.6 9.2 %reduce-scatter.3.cloned.1.call-done = bf16[16,16,2048]{2,1,0:T(8,128)(2,1)} async-done(((bf16[32,16,2048]{2,1,0:T(8,128)(2,1)}), bf16[16,16,2048]{2,1,0:T(8,128)(2,1)}) %reduce-scatter.3.cloned.1.call-update) | async-done | bytes 1048592 | tf_op jit(solution)/shard_map/reduce_scatter | solution.py:43
  224.9 1.4 copy.18
  226.3 74.6 %reduce-scatter.5.cloned.1.call-done = bf16[1,16,2048]{2,1,0:T(8,128)(2,1)} async-done(((bf16[16,16,2048]{2,1,0:T(8,128)(2,1)}), bf16[1,16,2048]{2,1,0:T(8,128)(2,1)}) %reduce-scatter.5.cloned.1.call-update) | async-done | bytes 65552 | tf_op jit(solution)/shard_map/reduce_scatter | solution.py:43
  (15 shorter events, 0.1 us)
Async XLA Ops:
  7.2 24.2 %copy-start.3 = (bf16[512,64]{0,1:T(8,128)(2,1)S(1)}, bf16[512,64]{0,1:T(8,128)(2,1)}, u32[]{:S(2)}) copy-start(bf16[512,64]{0,1:T(8,128)(2,1)} %param.5) | copy-start | bytes 196612
  32.9 15.6 %copy-start.1 = (f32[128,256]{1,0:T(8,128)S(1)}, f32[128,256]{1,0:T(8,128)}, u32[]{:S(2)}) copy-start(f32[128,256]{1,0:T(8,128)} %param.7) | copy-start | bytes 393220
  32.9 15.6 %copy-start.2 = (f32[128,256]{1,0:T(8,128)S(1)}, f32[128,256]{1,0:T(8,128)}, u32[]{:S(2)}) copy-start(f32[128,256]{1,0:T(8,128)} %param.8) | copy-start | bytes 393220
  32.9 15.6 %copy-start.4 = (f32[128]{0:T(128)S(1)}, f32[128]{0:T(128)}, u32[]{:S(2)}) copy-start(f32[128]{0:T(128)} %param.6) | copy-start | bytes 1540
  32.9 114.5 %all-to-all-start.2 = ((bf16[32,512,64]{1,2,0:T(8,128)(2,1)}), bf16[32,512,64]{1,2,0:T(8,128)(2,1)S(1)}, u32[]{:S(2)}, u32[]{:S(2)}) async-start(bf16[32,512,64]{1,2,0:T(8,128)(2,1)} %stack.2), calls=%async_computation.2 | async-start | bytes 4194304 | tf_op jit(solution)/shard_map/all_to_all | solution.py:62
  48.5 103.8 %all-gather.2.cloned.1.call-start = ((), (), s32[]{:S(2)}) async-start(), calls=%async_computation.5 | async-start | bytes 2228224 | tf_op jit(solution)/shard_map/all_gather | solution.py:15
  147.4 60.8 %all-to-all-start.1 = ((bf16[32,256,64]{1,2,0:T(8,128)(2,1)}), bf16[32,256,64]{1,2,0:T(8,128)(2,1)S(1)}, u32[]{:S(2)}, u32[]{:S(2)}) async-start(bf16[32,256,64]{1,2,0:T(8,128)(2,1)} %copy.16), calls=%async_computation.1 | async-start | bytes 2097152 | tf_op jit(solution)/shard_map/all_to_all | solution.py:70
  152.2 72.7 %reduce-scatter.3.cloned.1.call-start = ((), (), s32[]{:S(2)}) async-start(), calls=%async_computation.6 | async-start | bytes 3145728 | tf_op jit(solution)/shard_map/reduce_scatter | solution.py:43
  154.9 1.0 copy-start
  215.6 85.4 %reduce-scatter.5.cloned.1.call-start = ((), (), s32[]{:S(2)}) async-start(), calls=%async_computation.7 | async-start | bytes 1114112 | tf_op jit(solution)/shard_map/reduce_scatter | solution.py:43
Sparse Core Ops, SparseCore 0:
  52.9 58.0 all-gather.1
  215.7 9.1 reduce-scatter.2
  228.3 72.6 reduce-scatter.4
